TPU v7x, 32 devices: a whole 2x2x4 slice. The times are simulated.
32 devices in a mesh: dp: 4 (over y, x), kv: 4 (over z), tp: 2 (over core).
Axes of the slice: x: 2, y: 2, z: 4, core: 2. Of those that a mesh axis runs over, the one named last changes fastest.
Arguments:
- tokens: bfloat16 [32, 4096], P('dp', ('kv', 'tp')), may hold values from -7 to 7
- mix_gain: float32 [4096], replicated, may hold values from 0.1 to 1.9
- query_weight: bfloat16 [16, 128, 4096], P('tp', 'kv'), may hold values from -0.09375 to 0.09375
- forget_weight: bfloat16 [16, 128, 4096], P('tp', 'kv'), may hold values from -0.09375 to 0.09375
- value_weight: bfloat16 [16, 128, 4096], P('tp', 'kv'), may hold values from -0.09375 to 0.09375
- gate_weight: bfloat16 [16, 128, 4096], P('tp', 'kv'), may hold values from -0.09375 to 0.09375
- lower_bound: float32 [16, 128], P('tp'), may hold values from 0.02 to 0.9
- recurrent_state: float32 [32, 16, 128, 128], P(('dp', 'kv'), 'tp'), may hold values from -3 to 3
- head_gain: float32 [16, 128], P('tp'), may hold values from 0.1 to 1.9
- out_weight: bfloat16 [16, 128, 4096], P(None, None, ('kv', 'tp')), may hold values from -0.125 to 0.125
- mlp_gain: float32 [4096], replicated, may hold values from 0.1 to 1.9
- up_weight: bfloat16 [4096, 16384], P(None, ('kv', 'tp')), may hold values from -0.09375 to 0.09375
- down_weight: bfloat16 [16384, 4096], P(('kv', 'tp')), may hold values from -0.0625 to 0.0625
Outputs:
- layer_output: bfloat16 [32, 4096], P('dp', ('kv', 'tp'))
- next_state: float32 [32, 16, 128, 128], P(('dp', 'kv'), 'tp')
All inputs are finite; a program needn't handle non-finite values.
Results may differ from a plain program's by a relative error of at most 0.0072.
Values may be sent and summed in bfloat16 or wider, within the bound.
A program may use at most 128 MiB of HBM per device.

v0:
```python
import jax
import jax.numpy as jnp
from jax import lax
from jax.sharding import PartitionSpec as P

epsilon = 1e-06


def normed_rows(row_block, gain_vector):
    whole_rows = lax.all_gather(row_block, ("kv", "tp"), axis=1, tiled=True).astype(jnp.float32)
    inv_root = lax.rsqrt(jnp.mean(whole_rows * whole_rows, axis=1, keepdims=True) + epsilon)
    result_rows = (whole_rows * inv_root * gain_vector).astype(jnp.bfloat16)
    return result_rows


def local(
    tokens,
    mix_gain,
    query_weight,
    forget_weight,
    value_weight,
    gate_weight,
    lower_bound,
    recurrent_state,
    head_gain,
    out_weight,
    mlp_gain,
    up_weight,
    down_weight,
):
    normed = normed_rows(tokens, mix_gain)
    local_heads, local_chan, width = query_weight.shape
    stacked = jnp.stack((query_weight, forget_weight, value_weight, gate_weight), axis=0).reshape(
        -1, width
    )
    product = lax.dot_general(
        normed, stacked, (((1,), (1,)), ((), ())), preferred_element_type=jnp.float32
    ).astype(jnp.bfloat16)
    product = product.reshape(normed.shape[0], 4, local_heads, local_chan)
    pre_query, pre_forget, value_rows, pre_gate = (
        lax.all_to_all(product[:, 0], "kv", split_axis=0, concat_axis=2, tiled=True),
        lax.all_to_all(product[:, 1], "kv", split_axis=0, concat_axis=2, tiled=True),
        lax.all_to_all(product[:, 2], "kv", split_axis=0, concat_axis=2, tiled=True),
        lax.all_to_all(product[:, 3], "kv", split_axis=0, concat_axis=2, tiled=True),
    )
    log_forget = jnp.logaddexp(
        jnp.log(lower_bound),
        jnp.log1p(-lower_bound) + jax.nn.log_sigmoid(pre_forget.astype(jnp.float32)),
    )
    key_rows = -jnp.expm1(log_forget)
    next_state = (
        jnp.exp(log_forget)[:, :, :, None] * recurrent_state
        + key_rows[:, :, :, None] * value_rows.astype(jnp.float32)[:, :, None, :]
    )
    query_act = jax.nn.silu(pre_query.astype(jnp.float32))
    readout = jnp.einsum("bhk,bhkv->bhv", query_act, next_state, precision=lax.Precision.HIGHEST)
    inv_head = lax.rsqrt(jnp.mean(readout * readout, axis=2, keepdims=True) + epsilon)
    mixed_heads = (
        readout * inv_head * head_gain * jax.nn.silu(pre_gate.astype(jnp.float32))
    ).astype(jnp.bfloat16)
    all_heads = lax.all_gather(mixed_heads, "tp", axis=1, tiled=True)
    flat_mixed = all_heads.reshape(all_heads.shape[0], -1)
    out_matrix = out_weight.reshape(-1, out_weight.shape[2])
    projected = jnp.dot(
        lax.all_gather(flat_mixed, "kv", axis=0, tiled=True),
        out_matrix,
        preferred_element_type=jnp.float32,
    )
    residual = lax.optimization_barrier(
        (tokens.astype(jnp.float32) + projected).astype(jnp.bfloat16)
    )
    normed_mlp = normed_rows(residual, mlp_gain)
    hidden = jnp.square(
        jax.nn.relu(jnp.dot(normed_mlp, up_weight, preferred_element_type=jnp.float32))
    ).astype(jnp.bfloat16)
    summed = lax.psum_scatter(
        jnp.dot(hidden, down_weight, preferred_element_type=jnp.float32),
        ("kv", "tp"),
        scatter_dimension=1,
        tiled=True,
    )
    layer_output = (residual.astype(jnp.float32) + summed).astype(jnp.bfloat16)
    return (layer_output, next_state)


def solution(mesh):
    placed = (
        P("dp", ("kv", "tp")),
        P(),
        P("tp", "kv", None),
        P("tp", "kv", None),
        P("tp", "kv", None),
        P("tp", "kv", None),
        P("tp", None),
        P(("dp", "kv"), "tp", None, None),
        P("tp", None),
        P(None, None, ("kv", "tp")),
        P(),
        P(None, ("kv", "tp")),
        P(("kv", "tp"), None),
    )
    return jax.shard_map(
        local,
        mesh=mesh,
        in_specs=placed,
        out_specs=(P("dp", ("kv", "tp")), P(("dp", "kv"), "tp", None, None)),
        check_vma=False,
    )
```

profile of v0, /device:TPU:0, one launch (start us, length us, event | category | flops | bytes accessed | tf_op | source)
XLA Modules:
  0.0 148.9 jit_solution(8380039019351915380)
XLA Ops:
  7.2 16.0 %all_gather.12 = bf16[8,4096]{1,0:T(8,128)(2,1)S(1)} all-gather(bf16[8,512]{1,0:T(8,128)(2,1)} %param.13), channel_id=1, replica_groups=mesh['dp'=4,'kv'=4,'tp'=2] {'kv','tp'}, dimensions={1}, use_global_device_ids=true | all-gather | bytes 73728 | tf_op jit(solution)/shard_map/all_gather | solution.py:10
  23.4 4.4 %pad_maximum_fusion = bf16[4,8,32,4096]{3,2,1,0:T(8,128)(2,1)S(1)} fusion(bf16[1,8,32,4096]{3,2,1,0:T(8,128)(2,1)} %bitcast.47, bf16[1,8,32,4096]{3,2,1,0:T(8,128)(2,1)} %bitcast.48, bf16[1,8,32,4096]{3,2,1,0:T(8,128)(2,1)} %bitcast.49, bf16[1,8,32,4096]{3,2,1,0:T(8,128)(2,1)} %bitcast.50), kind=kLoop, calls=%fused_computation | loop fusion | flops 12582912 | bytes 16777216 | tf_op jit(solution)/shard_map/stack | solution.py:33
  27.8 2.3 %convolution_convert_fusion = bf16[8,1024]{1,0:T(8,128)(2,1)S(1)} fusion(bf16[1024,4096]{1,0:T(8,128)(2,1)S(1)} %bitcast.46, bf16[8,4096]{1,0:T(8,128)(2,1)S(1)} %all_gather.12, f32[4096]{0:T(1024)S(1)} %copy-done.3, f32[8]{0:T(128)S(1)} %add_rsqrt_fusion.2), kind=kOutput, calls=%fused_computation.4 | convolution fusion | flops 67248128 | bytes 8486944 | tf_op jit(solution)/shard_map/dot_general | solution.py:36
  30.2 0.7 reshape.119
  30.9 4.6 %all-to-all-start.1 = ((bf16[4,2,256]{2,1,0:T(2,128)(2,1)}), bf16[4,2,256]{2,1,0:T(2,128)(2,1)S(1)}, u32[]{:S(2)}, u32[]{:S(2)}) async-start(bf16[4,2,256]{2,1,0:T(2,128)(2,1)} %reshape.119), calls=%async_computation.1 | async-start | bytes 8192 | tf_op jit(solution)/shard_map/all_to_all | solution.py:42
  35.6 0.7 reshape.117
  36.2 0.7 reshape.115
  36.9 0.7 reshape.113
  37.6 3.5 %all-to-all-done.1 = bf16[4,2,256]{2,1,0:T(2,128)(2,1)S(1)} async-done(((bf16[4,2,256]{2,1,0:T(2,128)(2,1)}), bf16[4,2,256]{2,1,0:T(2,128)(2,1)S(1)}, u32[]{:S(2)}, u32[]{:S(2)}) %all-to-all-start.1) | async-done | bytes 4128 | tf_op jit(solution)/shard_map/all_to_all | solution.py:42
  41.1 3.2 %all-to-all-start.2 = ((bf16[4,2,256]{2,1,0:T(2,128)(2,1)}), bf16[4,2,256]{2,1,0:T(2,128)(2,1)S(1)}, u32[]{:S(2)}, u32[]{:S(2)}) async-start(bf16[4,2,256]{2,1,0:T(2,128)(2,1)} %reshape.117), calls=%async_computation.2 | async-start | bytes 8192 | tf_op jit(solution)/shard_map/all_to_all | solution.py:43
  44.4 5.4 %all-to-all-done.2 = bf16[4,2,256]{2,1,0:T(2,128)(2,1)S(1)} async-done(((bf16[4,2,256]{2,1,0:T(2,128)(2,1)}), bf16[4,2,256]{2,1,0:T(2,128)(2,1)S(1)}, u32[]{:S(2)}, u32[]{:S(2)}) %all-to-all-start.2) | async-done | bytes 4128 | tf_op jit(solution)/shard_map/all_to_all | solution.py:43
  49.9 3.2 %all-to-all-start = ((bf16[4,2,256]{2,1,0:T(2,128)(2,1)}), bf16[4,2,256]{2,1,0:T(2,128)(2,1)S(1)}, u32[]{:S(2)}, u32[]{:S(2)}) async-start(bf16[4,2,256]{2,1,0:T(2,128)(2,1)} %reshape.115), calls=%async_computation | async-start | bytes 8192 | tf_op jit(solution)/shard_map/all_to_all | solution.py:41
  53.4 5.2 %all-to-all-done = bf16[4,2,256]{2,1,0:T(2,128)(2,1)S(1)} async-done(((bf16[4,2,256]{2,1,0:T(2,128)(2,1)}), bf16[4,2,256]{2,1,0:T(2,128)(2,1)S(1)}, u32[]{:S(2)}, u32[]{:S(2)}) %all-to-all-start) | async-done | bytes 4128 | tf_op jit(solution)/shard_map/all_to_all | solution.py:41
  58.7 3.2 %all-to-all-start.3 = ((bf16[4,2,256]{2,1,0:T(2,128)(2,1)}), bf16[4,2,256]{2,1,0:T(2,128)(2,1)S(1)}, u32[]{:S(2)}, u32[]{:S(2)}) async-start(bf16[4,2,256]{2,1,0:T(2,128)(2,1)} %reshape.113), calls=%async_computation.3 | async-start | bytes 8192 | tf_op jit(solution)/shard_map/all_to_all | solution.py:44
  62.3 1.8 %multiply_add_fusion = f32[2,8,128,128]{3,2,1,0:T(8,128)S(1)} fusion(f32[2,8,128,128]{3,2,1,0:T(8,128)} %param.20, f32[2,8,128]{2,1,0:T(8,128)S(1)} %reshape.103, f32[2,8,128]{2,1,0:T(8,128)S(1)} %get-tuple-element.7, f32[2,8,128]{2,1,0:T(8,128)S(1)} %get-tuple-element.6), kind=kLoop, calls=%fused_computation.7 | loop fusion | flops 786432 | bytes 2121728 | tf_op jit(solution)/shard_map/add | solution.py:52
  64.1 1.0 fusion.25
  65.2 2.3 %all-to-all-done.3 = bf16[4,2,256]{2,1,0:T(2,128)(2,1)S(1)} async-done(((bf16[4,2,256]{2,1,0:T(2,128)(2,1)}), bf16[4,2,256]{2,1,0:T(2,128)(2,1)S(1)}, u32[]{:S(2)}, u32[]{:S(2)}) %all-to-all-start.3) | async-done | bytes 4128 | tf_op jit(solution)/shard_map/all_to_all | solution.py:44
  67.8 1.8 %all_gather.13 = bf16[2,16,128]{2,1,0:T(8,128)(2,1)S(1)} all-gather(bf16[2,8,128]{2,1,0:T(8,128)(2,1)S(1)} %multiply_convert_fusion), channel_id=1, replica_groups=mesh['dp'=4,'kv'=4,'tp'=2] {'tp'}, dimensions={1}, use_global_device_ids=true | all-gather | bytes 12288 | tf_op jit(solution)/shard_map/all_gather | solution.py:61
  69.6 13.1 %all-gather = bf16[4,2,2048]{2,1,0:T(2,128)(2,1)S(1)} all-gather(bf16[1,2,2048]{2,1,0:T(2,128)(2,1)S(1)} %reshape.108), channel_id=1, replica_groups=mesh['dp'=4,'kv'=4,'tp'=2] {'kv'}, dimensions={0}, use_global_device_ids=true | all-gather | bytes 40960 | tf_op jit(solution)/shard_map/all_gather | solution.py:65
  82.8 0.4 fusion.2
  83.2 14.0 %all_gather.15 = bf16[8,4096]{1,0:T(8,128)(2,1)S(1)} all-gather(bf16[8,512]{1,0:T(8,128)(2,1)S(1)} %fusion.2), channel_id=1, replica_groups=mesh['dp'=4,'kv'=4,'tp'=2] {'kv','tp'}, dimensions={1}, use_global_device_ids=true | all-gather | bytes 73728 | tf_op jit(solution)/shard_map/all_gather | solution.py:10
  97.3 13.5 %fusion.3 = f32[8,4096]{1,0:T(8,128)} fusion(bf16[2048,4096]{1,0:T(8,128)(2,1)} %param.25, bf16[4096,2048]{1,0:T(8,128)(2,1)} %param.24, bf16[8,4096]{1,0:T(8,128)(2,1)S(1)} %all_gather.15, f32[4096]{0:T(1024)S(1)} %copy-done.4, f32[8]{0:T(128)S(1)} %add_rsqrt_fusion.1), kind=kOutput, calls=%fused_computation.8 | convolution fusion | flops 268615680 | bytes 33767456 | tf_op jit(solution)/shard_map/dot_general | solution.py:77
  110.9 29.9 %reduce-scatter.2.cloned.1.call-done = f32[8,512]{1,0:T(8,128)} async-done(((f32[8,4096]{1,0:T(8,128)}), f32[8,512]{1,0:T(8,128)}) %reduce-scatter.2.cloned.1.call-update) | async-done | bytes 16400 | tf_op jit(solution)/shard_map/reduce_scatter | solution.py:76
  140.7 1.3 add_convert_fusion
  (46 shorter events, 1.6 us)
Async XLA Ops:
  7.2 75.6 %copy-start = (bf16[16,128,512]{2,1,0:T(8,128)(2,1)S(1)}, bf16[16,128,512]{2,1,0:T(8,128)(2,1)}, u32[]{:S(2)}) copy-start(bf16[16,128,512]{2,1,0:T(8,128)(2,1)} %param.22) | copy-start | bytes 6291460
  23.4 4.4 %copy-start.3 = (f32[4096]{0:T(1024)S(1)}, f32[4096]{0:T(1024)}, u32[]{:S(2)}) copy-start(f32[4096]{0:T(1024)} %param.14) | copy-start | bytes 49156
  27.7 7.8 %copy-start.5 = (f32[8,128]{1,0:T(8,128)S(1)}, f32[8,128]{1,0:T(8,128)}, u32[]{:S(2)}) copy-start(f32[8,128]{1,0:T(8,128)} %param.19) | copy-start | bytes 12292
  27.8 39.9 %copy-start.6 = (f32[8,128]{1,0:T(8,128)S(1)}, f32[8,128]{1,0:T(8,128)}, u32[]{:S(2)}) copy-start(f32[8,128]{1,0:T(8,128)} %param.21) | copy-start | bytes 12292
  27.8 55.0 %copy-start.2 = (bf16[8,512]{1,0:T(8,128)(2,1)S(1)}, bf16[8,512]{1,0:T(8,128)(2,1)}, u32[]{:S(2)}) copy-start(bf16[8,512]{1,0:T(8,128)(2,1)} %param.13) | copy-start | bytes 24580
  27.8 69.5 %copy-start.4 = (f32[4096]{0:T(1024)S(1)}, f32[4096]{0:T(1024)}, u32[]{:S(2)}) copy-start(f32[4096]{0:T(1024)} %param.23) | copy-start | bytes 49156
  30.9 10.2 %all-to-all-start.1 = ((bf16[4,2,256]{2,1,0:T(2,128)(2,1)}), bf16[4,2,256]{2,1,0:T(2,128)(2,1)S(1)}, u32[]{:S(2)}, u32[]{:S(2)}) async-start(bf16[4,2,256]{2,1,0:T(2,128)(2,1)} %reshape.119), calls=%async_computation.1 | async-start | bytes 8192 | tf_op jit(solution)/shard_map/all_to_all | solution.py:42
  41.1 8.8 %all-to-all-start.2 = ((bf16[4,2,256]{2,1,0:T(2,128)(2,1)}), bf16[4,2,256]{2,1,0:T(2,128)(2,1)S(1)}, u32[]{:S(2)}, u32[]{:S(2)}) async-start(bf16[4,2,256]{2,1,0:T(2,128)(2,1)} %reshape.117), calls=%async_computation.2 | async-start | bytes 8192 | tf_op jit(solution)/shard_map/all_to_all | solution.py:43
  49.9 8.8 %all-to-all-start = ((bf16[4,2,256]{2,1,0:T(2,128)(2,1)}), bf16[4,2,256]{2,1,0:T(2,128)(2,1)S(1)}, u32[]{:S(2)}, u32[]{:S(2)}) async-start(bf16[4,2,256]{2,1,0:T(2,128)(2,1)} %reshape.115), calls=%async_computation | async-start | bytes 8192 | tf_op jit(solution)/shard_map/all_to_all | solution.py:41
  58.7 8.8 %all-to-all-start.3 = ((bf16[4,2,256]{2,1,0:T(2,128)(2,1)}), bf16[4,2,256]{2,1,0:T(2,128)(2,1)S(1)}, u32[]{:S(2)}, u32[]{:S(2)}) async-start(bf16[4,2,256]{2,1,0:T(2,128)(2,1)} %reshape.113), calls=%async_computation.3 | async-start | bytes 8192 | tf_op jit(solution)/shard_map/all_to_all | solution.py:44
  61.9 78.8 %reduce-scatter.2.cloned.1.call-start = ((), (), s32[]{:S(2)}) async-start(), calls=%async_computation.5 | async-start | bytes 147456 | tf_op jit(solution)/shard_map/reduce_scatter | solution.py:76
  64.1 46.7 %copy-start.1 = (f32[2,8,128,128]{3,2,1,0:T(8,128)}, f32[2,8,128,128]{3,2,1,0:T(8,128)S(1)}, u32[]{:S(2)}) copy-start(f32[2,8,128,128]{3,2,1,0:T(8,128)S(1)} %multiply_add_fusion) | copy-start | bytes 3145732
Sparse Core Ops, SparseCore 0:
  111.0 29.6 reduce-scatter.1
where the time goes:
time: 149 us
  waiting for transfers between devices  46.4 us (31%)
  blocking collectives  45 us (30%)
  matrix products  17.1 us (11%)
  starting transfers between devices  14.4 us (10%)
  between operations  14.2 us (10%)
  other arithmetic  8.09 us (5%)
  local copies, waits for them, and re-layouts  3.68 us (2%)
    all_gather x2, blocking collectives, normed_rows(): lax.all_gather(row_block, ('kv', 'tp'), axis=1, tiled=True)  30 us
    reduce_scatter x1, waiting for transfers between devices, local(): lax.psum_scatter(jnp.dot(hidden, down_weight, preferred_element_type=jnp....  29.9 us
    dot_general x1, matrix products, local(): jnp.dot(hidden, down_weight, preferred_element_type=jnp.float32)  13.5 us
    all_gather x1, blocking collectives, local(): lax.all_gather(flat_mixed, 'kv', axis=0, tiled=True)  13.1 us
    all_to_all x1, waiting for transfers between devices, local(): lax.all_to_all(product[:, 2], 'kv', split_axis=0, concat_axis=2, tiled=True)  5.45 us
    all_to_all x1, waiting for transfers between devices, local(): lax.all_to_all(product[:, 0], 'kv', split_axis=0, concat_axis=2, tiled=True)  5.25 us
    all_to_all x1, starting transfers between devices, local(): lax.all_to_all(product[:, 1], 'kv', split_axis=0, concat_axis=2, tiled=True)  4.64 us
    another operation x1, other arithmetic, local(): jnp.stack((query_weight, forget_weight, value_weight, gate_weight), axis=0)  4.36 us
  transfers between devices with their start and end apart: 5, of which 5 were waited for; matrix products, arithmetic and copies ran while one was open for 4% of the time, Pallas kernels for 0%

commit v1 on v0

--- a/solution.py
+++ b/solution.py
@@ -61,10 +61,22 @@
     all_heads = lax.all_gather(mixed_heads, "tp", axis=1, tiled=True)
     flat_mixed = all_heads.reshape(all_heads.shape[0], -1)
     out_matrix = out_weight.reshape(-1, out_weight.shape[2])
+
+    def wires_start(mat, axis_id):
+        b_now = lax.axis_size(axis_id)
+        r2 = lax.axis_index(axis_id)
+        current_block, vec_out = (b_now, r2)
+        h_now, r1 = (mat, 1)
+        while r1 < current_block:
+            front = lax.ppermute(h_now, axis_id, [(j, j ^ r1) for j in range(current_block)])
+            tile_out = jnp.concatenate([h_now, front], 0)
+            o_now = jnp.concatenate([front, h_now], 0)
+            h_now = jnp.where(vec_out & r1 == 0, tile_out, o_now)
+            r1 = 2 * r1
+        return h_now
+
     projected = jnp.dot(
-        lax.all_gather(flat_mixed, "kv", axis=0, tiled=True),
-        out_matrix,
-        preferred_element_type=jnp.float32,
+        wires_start(flat_mixed, "kv"), out_matrix, preferred_element_type=jnp.float32
     )
     residual = lax.optimization_barrier(
         (tokens.astype(jnp.float32) + projected).astype(jnp.bfloat16)

time: 149 us -> 145 us (0.973)
  blocking collectives: 45 us -> 31.9 us
  waiting for transfers between devices: 46.4 us -> 53.7 us
    all_gather x1 -> x0, blocking collectives: 13.1 us -> none  [local(): lax.all_gather(flat_mixed, 'kv', axis=0, tiled=True)]
    ppermute x0 -> x2, waiting for transfers between devices: none -> 7.3 us  [wires_start(): lax.ppermute(h_now, axis_id, [(j, j ^ r1) for j in range(current_block)])]
    unnamed x24 -> x23, local copies, waits for them, and re-layouts: 3.14 us -> 3.11 us
  transfers between devices with their start and end apart: 5 -> 7, of which waited for: 5 -> 7; matrix products, arithmetic and copies ran while one was open for 4% -> 4% of each run, Pallas kernels for 0% -> 0%
where the time goes in v1:
time: 145 us; the launch traced here: 144 us
  waiting for transfers between devices  53.7 us (37%)
  blocking collectives  31.9 us (22%)
  matrix products  17.1 us (12%)
  starting transfers between devices  15.7 us (11%)
  between operations  14.2 us (10%)
  other arithmetic  8.13 us (6%)
  local copies, waits for them, and re-layouts  3.65 us (3%)
    all_gather x2, blocking collectives, normed_rows(): lax.all_gather(row_block, ('kv', 'tp'), axis=1, tiled=True)  30 us
    reduce_scatter x1, waiting for transfers between devices, local(): lax.psum_scatter(jnp.dot(hidden, down_weight, preferred_element_type=jnp....  29.8 us
    dot_general x1, matrix products, local(): jnp.dot(hidden, down_weight, preferred_element_type=jnp.float32)  13.5 us
    ppermute x2, waiting for transfers between devices, wires_start(): lax.ppermute(h_now, axis_id, [(j, j ^ r1) for j in range(current_block)])  7.3 us
    all_to_all x1, waiting for transfers between devices, local(): lax.all_to_all(product[:, 2], 'kv', split_axis=0, concat_axis=2, tiled=True)  5.45 us
    all_to_all x1, waiting for transfers between devices, local(): lax.all_to_all(product[:, 0], 'kv', split_axis=0, concat_axis=2, tiled=True)  5.25 us
    all_to_all x1, starting transfers between devices, local(): lax.all_to_all(product[:, 1], 'kv', split_axis=0, concat_axis=2, tiled=True)  4.64 us
    another operation x1, other arithmetic, local(): jnp.stack((query_weight, forget_weight, value_weight, gate_weight), axis=0)  4.36 us
  transfers between devices with their start and end apart: 7, of which 7 were waited for; matrix products, arithmetic and copies ran while one was open for 4% of the time, Pallas kernels for 0%

profile of v1, /device:TPU:0, one launch (start us, length us, event | category | flops | bytes accessed | tf_op | source)
XLA Modules:
  0.0 144.3 jit_solution(8344701690101081109)
XLA Ops:
  7.2 16.0 %all_gather.9 = bf16[8,4096]{1,0:T(8,128)(2,1)S(1)} all-gather(bf16[8,512]{1,0:T(8,128)(2,1)} %param.13), channel_id=1, replica_groups=mesh['dp'=4,'kv'=4,'tp'=2] {'kv','tp'}, dimensions={1}, use_global_device_ids=true | all-gather | bytes 73728 | tf_op jit(solution)/shard_map/all_gather | solution.py:10
  23.4 4.4 %pad_maximum_fusion = bf16[4,8,32,4096]{3,2,1,0:T(8,128)(2,1)S(1)} fusion(bf16[1,8,32,4096]{3,2,1,0:T(8,128)(2,1)} %bitcast.50, bf16[1,8,32,4096]{3,2,1,0:T(8,128)(2,1)} %bitcast.51, bf16[1,8,32,4096]{3,2,1,0:T(8,128)(2,1)} %bitcast.52, bf16[1,8,32,4096]{3,2,1,0:T(8,128)(2,1)} %bitcast.53), kind=kLoop, calls=%fused_computation | loop fusion | flops 12582912 | bytes 16777216 | tf_op jit(solution)/shard_map/stack | solution.py:33
  27.8 2.3 %convolution_convert_fusion = bf16[8,1024]{1,0:T(8,128)(2,1)S(1)} fusion(bf16[1024,4096]{1,0:T(8,128)(2,1)S(1)} %bitcast.49, bf16[8,4096]{1,0:T(8,128)(2,1)S(1)} %all_gather.9, f32[4096]{0:T(1024)S(1)} %copy-done.3, f32[8]{0:T(128)S(1)} %add_rsqrt_fusion.2), kind=kOutput, calls=%fused_computation.4 | convolution fusion | flops 67248128 | bytes 8486944 | tf_op jit(solution)/shard_map/dot_general | solution.py:36
  30.2 0.7 reshape.116
  30.9 4.6 %all-to-all-start.1 = ((bf16[4,2,256]{2,1,0:T(2,128)(2,1)}), bf16[4,2,256]{2,1,0:T(2,128)(2,1)S(1)}, u32[]{:S(2)}, u32[]{:S(2)}) async-start(bf16[4,2,256]{2,1,0:T(2,128)(2,1)} %reshape.116), calls=%async_computation.1 | async-start | bytes 8192 | tf_op jit(solution)/shard_map/all_to_all | solution.py:42
  35.5 0.7 reshape.114
  36.2 0.7 reshape.112
  36.9 0.7 reshape.110
  37.6 3.5 %all-to-all-done.1 = bf16[4,2,256]{2,1,0:T(2,128)(2,1)S(1)} async-done(((bf16[4,2,256]{2,1,0:T(2,128)(2,1)}), bf16[4,2,256]{2,1,0:T(2,128)(2,1)S(1)}, u32[]{:S(2)}, u32[]{:S(2)}) %all-to-all-start.1) | async-done | bytes 4128 | tf_op jit(solution)/shard_map/all_to_all | solution.py:42
  41.1 3.2 %all-to-all-start.2 = ((bf16[4,2,256]{2,1,0:T(2,128)(2,1)}), bf16[4,2,256]{2,1,0:T(2,128)(2,1)S(1)}, u32[]{:S(2)}, u32[]{:S(2)}) async-start(bf16[4,2,256]{2,1,0:T(2,128)(2,1)} %reshape.114), calls=%async_computation.2 | async-start | bytes 8192 | tf_op jit(solution)/shard_map/all_to_all | solution.py:43
  44.5 5.4 %all-to-all-done.2 = bf16[4,2,256]{2,1,0:T(2,128)(2,1)S(1)} async-done(((bf16[4,2,256]{2,1,0:T(2,128)(2,1)}), bf16[4,2,256]{2,1,0:T(2,128)(2,1)S(1)}, u32[]{:S(2)}, u32[]{:S(2)}) %all-to-all-start.2) | async-done | bytes 4128 | tf_op jit(solution)/shard_map/all_to_all | solution.py:43
  49.9 3.2 %all-to-all-start = ((bf16[4,2,256]{2,1,0:T(2,128)(2,1)}), bf16[4,2,256]{2,1,0:T(2,128)(2,1)S(1)}, u32[]{:S(2)}, u32[]{:S(2)}) async-start(bf16[4,2,256]{2,1,0:T(2,128)(2,1)} %reshape.112), calls=%async_computation | async-start | bytes 8192 | tf_op jit(solution)/shard_map/all_to_all | solution.py:41
  53.5 5.2 %all-to-all-done = bf16[4,2,256]{2,1,0:T(2,128)(2,1)S(1)} async-done(((bf16[4,2,256]{2,1,0:T(2,128)(2,1)}), bf16[4,2,256]{2,1,0:T(2,128)(2,1)S(1)}, u32[]{:S(2)}, u32[]{:S(2)}) %all-to-all-start) | async-done | bytes 4128 | tf_op jit(solution)/shard_map/all_to_all | solution.py:41
  58.7 3.2 %all-to-all-start.3 = ((bf16[4,2,256]{2,1,0:T(2,128)(2,1)}), bf16[4,2,256]{2,1,0:T(2,128)(2,1)S(1)}, u32[]{:S(2)}, u32[]{:S(2)}) async-start(bf16[4,2,256]{2,1,0:T(2,128)(2,1)} %reshape.110), calls=%async_computation.3 | async-start | bytes 8192 | tf_op jit(solution)/shard_map/all_to_all | solution.py:44
  62.3 1.8 %multiply_add_fusion = f32[2,8,128,128]{3,2,1,0:T(8,128)S(1)} fusion(f32[2,8,128,128]{3,2,1,0:T(8,128)} %param.20, f32[2,8,128]{2,1,0:T(8,128)S(1)} %reshape.103, f32[2,8,128]{2,1,0:T(8,128)S(1)} %get-tuple-element.7, f32[2,8,128]{2,1,0:T(8,128)S(1)} %get-tuple-element.6), kind=kLoop, calls=%fused_computation.7 | loop fusion | flops 786432 | bytes 2121728 | tf_op jit(solution)/shard_map/add | solution.py:52
  64.1 1.0 fusion.32
  65.2 2.3 %all-to-all-done.3 = bf16[4,2,256]{2,1,0:T(2,128)(2,1)S(1)} async-done(((bf16[4,2,256]{2,1,0:T(2,128)(2,1)}), bf16[4,2,256]{2,1,0:T(2,128)(2,1)S(1)}, u32[]{:S(2)}, u32[]{:S(2)}) %all-to-all-start.3) | async-done | bytes 4128 | tf_op jit(solution)/shard_map/all_to_all | solution.py:44
  67.8 1.8 %all_gather.10 = bf16[2,16,128]{2,1,0:T(8,128)(2,1)S(1)} all-gather(bf16[2,8,128]{2,1,0:T(8,128)(2,1)S(1)} %multiply_convert_fusion), channel_id=1, replica_groups=mesh['dp'=4,'kv'=4,'tp'=2] {'tp'}, dimensions={1}, use_global_device_ids=true | all-gather | bytes 12288 | tf_op jit(solution)/shard_map/all_gather | solution.py:61
  70.3 3.1 %collective-permute-done = bf16[2,2048]{1,0:T(2,128)(2,1)S(1)} collective-permute-done((bf16[2,2048]{1,0:T(2,128)(2,1)S(1)}, bf16[2,2048]{1,0:T(2,128)(2,1)S(1)}, u32[]{:S(2)}, u32[]{:S(2)}) %collective-permute-start) | collective-permute-done | bytes 8224 | tf_op jit(solution)/shard_map/ppermute | solution.py:71
  74.0 4.2 %collective-permute-done.1 = bf16[4,2048]{1,0:T(4,128)(2,1)S(1)} collective-permute-done((bf16[4,2048]{1,0:T(4,128)(2,1)S(1)}, bf16[4,2048]{1,0:T(4,128)(2,1)S(1)}, u32[]{:S(2)}, u32[]{:S(2)}) %collective-permute-start.1) | collective-permute-done | bytes 16416 | tf_op jit(solution)/shard_map/ppermute | solution.py:71
  78.6 14.0 %all_gather.11 = bf16[8,4096]{1,0:T(8,128)(2,1)S(1)} all-gather(bf16[8,512]{1,0:T(8,128)(2,1)S(1)} %fusion.2), channel_id=1, replica_groups=mesh['dp'=4,'kv'=4,'tp'=2] {'kv','tp'}, dimensions={1}, use_global_device_ids=true | all-gather | bytes 73728 | tf_op jit(solution)/shard_map/all_gather | solution.py:10
  92.8 13.5 %fusion.3 = f32[8,4096]{1,0:T(8,128)} fusion(bf16[2048,4096]{1,0:T(8,128)(2,1)} %param.25, bf16[4096,2048]{1,0:T(8,128)(2,1)} %param.24, bf16[8,4096]{1,0:T(8,128)(2,1)S(1)} %all_gather.11, f32[4096]{0:T(1024)S(1)} %copy-done.4, f32[8]{0:T(128)S(1)} %add_rsqrt_fusion.1), kind=kOutput, calls=%fused_computation.8 | convolution fusion | flops 268615680 | bytes 33767456 | tf_op jit(solution)/shard_map/dot_general | solution.py:89
  106.3 29.8 %reduce-scatter.2.cloned.1.call-done = f32[8,512]{1,0:T(8,128)} async-done(((f32[8,4096]{1,0:T(8,128)}), f32[8,512]{1,0:T(8,128)}) %reduce-scatter.2.cloned.1.call-update) | async-done | bytes 16400 | tf_op jit(solution)/shard_map/reduce_scatter | solution.py:88
  136.2 1.3 add_convert_fusion
  (49 shorter events, 3.3 us)
Async XLA Ops:
  7.2 71.1 %copy-start = (bf16[16,128,512]{2,1,0:T(8,128)(2,1)S(1)}, bf16[16,128,512]{2,1,0:T(8,128)(2,1)}, u32[]{:S(2)}) copy-start(bf16[16,128,512]{2,1,0:T(8,128)(2,1)} %param.22) | copy-start | bytes 6291460
  23.4 4.4 %copy-start.3 = (f32[4096]{0:T(1024)S(1)}, f32[4096]{0:T(1024)}, u32[]{:S(2)}) copy-start(f32[4096]{0:T(1024)} %param.14) | copy-start | bytes 49156
  27.7 7.8 %copy-start.5 = (f32[8,128]{1,0:T(8,128)S(1)}, f32[8,128]{1,0:T(8,128)}, u32[]{:S(2)}) copy-start(f32[8,128]{1,0:T(8,128)} %param.19) | copy-start | bytes 12292
  27.8 40.0 %copy-start.6 = (f32[8,128]{1,0:T(8,128)S(1)}, f32[8,128]{1,0:T(8,128)}, u32[]{:S(2)}) copy-start(f32[8,128]{1,0:T(8,128)} %param.21) | copy-start | bytes 12292
  27.8 50.5 %copy-start.2 = (bf16[8,512]{1,0:T(8,128)(2,1)S(1)}, bf16[8,512]{1,0:T(8,128)(2,1)}, u32[]{:S(2)}) copy-start(bf16[8,512]{1,0:T(8,128)(2,1)} %param.13) | copy-start | bytes 24580
  27.8 65.0 %copy-start.4 = (f32[4096]{0:T(1024)S(1)}, f32[4096]{0:T(1024)}, u32[]{:S(2)}) copy-start(f32[4096]{0:T(1024)} %param.23) | copy-start | bytes 49156
  30.9 10.2 %all-to-all-start.1 = ((bf16[4,2,256]{2,1,0:T(2,128)(2,1)}), bf16[4,2,256]{2,1,0:T(2,128)(2,1)S(1)}, u32[]{:S(2)}, u32[]{:S(2)}) async-start(bf16[4,2,256]{2,1,0:T(2,128)(2,1)} %reshape.116), calls=%async_computation.1 | async-start | bytes 8192 | tf_op jit(solution)/shard_map/all_to_all | solution.py:42
  41.1 8.8 %all-to-all-start.2 = ((bf16[4,2,256]{2,1,0:T(2,128)(2,1)}), bf16[4,2,256]{2,1,0:T(2,128)(2,1)S(1)}, u32[]{:S(2)}, u32[]{:S(2)}) async-start(bf16[4,2,256]{2,1,0:T(2,128)(2,1)} %reshape.114), calls=%async_computation.2 | async-start | bytes 8192 | tf_op jit(solution)/shard_map/all_to_all | solution.py:43
  49.9 8.8 %all-to-all-start = ((bf16[4,2,256]{2,1,0:T(2,128)(2,1)}), bf16[4,2,256]{2,1,0:T(2,128)(2,1)S(1)}, u32[]{:S(2)}, u32[]{:S(2)}) async-start(bf16[4,2,256]{2,1,0:T(2,128)(2,1)} %reshape.112), calls=%async_computation | async-start | bytes 8192 | tf_op jit(solution)/shard_map/all_to_all | solution.py:41
  58.7 8.8 %all-to-all-start.3 = ((bf16[4,2,256]{2,1,0:T(2,128)(2,1)}), bf16[4,2,256]{2,1,0:T(2,128)(2,1)S(1)}, u32[]{:S(2)}, u32[]{:S(2)}) async-start(bf16[4,2,256]{2,1,0:T(2,128)(2,1)} %reshape.110), calls=%async_computation.3 | async-start | bytes 8192 | tf_op jit(solution)/shard_map/all_to_all | solution.py:44
  62.0 74.2 %reduce-scatter.2.cloned.1.call-start = ((), (), s32[]{:S(2)}) async-start(), calls=%async_computation.5 | async-start | bytes 147456 | tf_op jit(solution)/shard_map/reduce_scatter | solution.py:88
  64.1 42.2 %copy-start.1 = (f32[2,8,128,128]{3,2,1,0:T(8,128)}, f32[2,8,128,128]{3,2,1,0:T(8,128)S(1)}, u32[]{:S(2)}) copy-start(f32[2,8,128,128]{3,2,1,0:T(8,128)S(1)} %multiply_add_fusion) | copy-start | bytes 3145732
  69.6 3.7 %collective-permute-start = (bf16[2,2048]{1,0:T(2,128)(2,1)S(1)}, bf16[2,2048]{1,0:T(2,128)(2,1)S(1)}, u32[]{:S(2)}, u32[]{:S(2)}) collective-permute-start(bf16[2,2048]{1,0:T(2,128)(2,1)S(1)} %bitcast.62), channel_id=1, source_target_pairs={{0,2},{2,0},{4,6},{6,4},{1,3},{3,1},{5,7},{7,5},{8,10},{10,8},{12,... | collective-permute-start | bytes 24584 | tf_op jit(solution)/shard_map/ppermute | solution.py:71
  73.4 4.9 %collective-permute-start.1 = (bf16[4,2048]{1,0:T(4,128)(2,1)S(1)}, bf16[4,2048]{1,0:T(4,128)(2,1)S(1)}, u32[]{:S(2)}, u32[]{:S(2)}) collective-permute-start(bf16[4,2048]{1,0:T(4,128)(2,1)S(1)} %maximum_select_fusion.2), channel_id=1, source_target_pairs={{0,4},{2,6},{4,0},{6,2},{1,5},{3,7},{5,1},{7,3},{8,12},{10,14},{12... | collective-permute-start | bytes 49160 | tf_op jit(solution)/shard_map/ppermute | solution.py:71
Sparse Core Ops, SparseCore 0:
  106.5 29.6 reduce-scatter.1
